TPU v7x, 32 devices: a whole 2x2x4 slice. The times are simulated.
32 devices in a mesh: ep: 4 (over y, x), tp: 8 (over z, core).
Axes of the slice: x: 2, y: 2, z: 4, core: 2. Of those that a mesh axis runs over, the one named last changes fastest.
Arguments:
- tokens: bfloat16 [64, 4096], P(None, 'ep'), may hold values from -60 to 60
- gain_attn: bfloat16 [4096], P('ep'), may hold values from 0.099609375 to 1.8984375
- w_query: bfloat16 [4096, 2048], P('ep', 'tp'), may hold values from -0.09375 to 0.09375
- w_key: bfloat16 [4096, 2048], P('ep', 'tp'), may hold values from -0.09375 to 0.09375
- w_value: bfloat16 [4096, 2048], P('ep', 'tp'), may hold values from -0.09375 to 0.09375
- w_output: bfloat16 [2048, 4096], P('tp', 'ep'), may hold values from -0.125 to 0.125
- key_cache: bfloat16 [64, 1024, 2048], P('ep', None, 'tp'), may hold values from -6 to 6
- value_cache: bfloat16 [64, 1024, 2048], P('ep', None, 'tp'), may hold values from -10 to 10
- lengths: int32 [64], P('ep'), may hold values from 128 to 1024
- score_shift: float32 [16], P('tp'), may hold values from -9.5 to -3.5
- gain_ffn: bfloat16 [4096], replicated, may hold values from 0.099609375 to 1.8984375
- w_mix: bfloat16 [4096], P('ep'), may hold values from -0.09375 to 0.09375
- w_dense_gate: bfloat16 [4096, 4096], P('ep', 'tp'), may hold values from -0.09375 to 0.09375
- w_dense_up: bfloat16 [4096, 4096], P('ep', 'tp'), may hold values from -0.09375 to 0.09375
- w_dense_down: bfloat16 [4096, 4096], P('tp', 'ep'), may hold values from -0.09375 to 0.09375
- route_group: int32 [64], replicated, may hold values from 0 to 3, as said below
- route_inner: int32 [64, 2], replicated, may hold values from 0 to 3, as said below
- route_weight: float32 [64, 2], replicated, may hold values from 0.3 to 1
- w_exp_gate: bfloat16 [16, 4096, 2048], P('ep', None, 'tp'), may hold values from -0.09375 to 0.09375
- w_exp_up: bfloat16 [16, 4096, 2048], P('ep', None, 'tp'), may hold values from -0.09375 to 0.09375
- w_exp_down: bfloat16 [16, 2048, 4096], P('ep', 'tp'), may hold values from -0.125 to 0.125
Outputs:
- mixed: bfloat16 [64, 4096], P(None, 'ep')
- new_keys: bfloat16 [64, 2048], P('ep', 'tp')
- new_values: bfloat16 [64, 2048], P('ep', 'tp')
Inputs may be any that keep to these rules, and one draw needn't show every extreme that they name: `route_group`: within every aligned block of 16 sequences (the sequences of one index of ep) exactly half of the tokens use one group, the same group in every block; the other groups share the rest. A token's 2 experts inside its group differ. Within every aligned block of 16 sequences no expert (route_group * 4 + route_inner) is used by more than 4 tokens, and the experts of the group that half of the block uses are each used by exactly 4.
All inputs are finite; a program needn't handle non-finite values.
Results may differ from a plain program's by a relative error of at most 0.0039.
The roundings to bfloat16 on the way count: a program that leaves them out, or rounds other values in their place, can miss the bound.
Values may be sent and summed in bfloat16 or wider, within the bound.
A program may use at most 128 MiB of HBM per device.

v0:
```python
import math
import jax
import jax.numpy as jnp
from jax import lax
from jax.sharding import PartitionSpec as P

D = 4096
HD = 128
EPG = 4
TOPK = 2
EXPERTS = 16
CAP = 4
norm_eps = 1e-06


def on_device(
    tokens,
    gain_attn,
    w_query,
    w_key,
    w_value,
    w_output,
    key_cache,
    value_cache,
    lengths,
    score_shift,
    gain_ffn,
    w_mix,
    w_dense_gate,
    w_dense_up,
    w_dense_down,
    route_group,
    route_inner,
    route_weight,
    w_exp_gate,
    w_exp_up,
    w_exp_down,
):
    ep_count = lax.axis_size("ep")
    batch_all, col_width = tokens.shape
    seq_local = batch_all // ep_count
    head_cols = w_query.shape[1]
    heads_local = head_cols // HD
    tokens_float = tokens.astype(jnp.float32)
    squares = lax.psum_scatter(
        jnp.sum(tokens_float * tokens_float, axis=1), "ep", scatter_dimension=0, tiled=True
    )
    inv_first = lax.rsqrt(squares / D + norm_eps)[:, None]
    scaled_in = (tokens_float * gain_attn.astype(jnp.float32)).astype(jnp.bfloat16)
    w_joint = jnp.concatenate([w_query, w_key, w_value], axis=1)
    joint_proj = (
        lax.psum_scatter(
            jnp.dot(scaled_in, w_joint, preferred_element_type=jnp.float32),
            "ep",
            scatter_dimension=0,
            tiled=True,
        )
        * inv_first
    )
    queries = joint_proj[:, :head_cols].astype(jnp.bfloat16)
    new_keys = joint_proj[:, head_cols : 2 * head_cols].astype(jnp.bfloat16)
    new_values = joint_proj[:, 2 * head_cols :].astype(jnp.bfloat16)
    cache_len = key_cache.shape[1]
    head_query = queries.reshape(seq_local, heads_local, HD)
    head_keys = key_cache.reshape(seq_local, cache_len, heads_local, HD)
    scores = jnp.einsum(
        "bhd,blhd->bhl", head_query, head_keys, preferred_element_type=jnp.float32
    ) / math.sqrt(HD)
    scores = scores + score_shift[None, :, None]
    live_mask = lax.broadcasted_iota(jnp.int32, scores.shape, 2) < lengths[:, None, None]
    soft_terms = jnp.where(live_mask, jax.nn.softplus(scores), 0.0)
    later_sum = lax.cumsum(soft_terms, axis=2, reverse=True) - soft_terms
    stick = jnp.where(live_mask, jnp.exp(jax.nn.log_sigmoid(scores) - later_sum), 0.0).astype(
        jnp.bfloat16
    )
    head_values = value_cache.reshape(seq_local, cache_len, heads_local, HD)
    attended = jnp.einsum("bhl,blhd->bhd", stick, head_values, preferred_element_type=jnp.float32)
    attended = attended.reshape(seq_local, head_cols).astype(jnp.bfloat16)
    attn_part = jnp.dot(
        lax.all_gather(attended, "ep", axis=0, tiled=True),
        w_output,
        preferred_element_type=jnp.float32,
    )
    attn_out = lax.psum(attn_part, "tp")
    middle = (tokens_float + attn_out).astype(jnp.bfloat16)
    middle_float = middle.astype(jnp.float32)
    gain_float = gain_ffn.astype(jnp.float32)
    gain_cols = lax.dynamic_slice_in_dim(gain_float, lax.axis_index("ep") * col_width, col_width, 0)
    scaled_mid = (middle_float * gain_cols).astype(jnp.bfloat16)
    dense_pre, dense_lin, mix_pre, mid_squares = lax.psum(
        (
            jnp.dot(scaled_mid, w_dense_gate, preferred_element_type=jnp.float32),
            jnp.dot(scaled_mid, w_dense_up, preferred_element_type=jnp.float32),
            jnp.dot(scaled_mid, w_mix, preferred_element_type=jnp.float32),
            jnp.sum(middle_float * middle_float, axis=1),
        ),
        "ep",
    )
    inv_second = lax.rsqrt(mid_squares / D + norm_eps)[:, None]
    dense_hidden = (jax.nn.silu(dense_pre * inv_second) * (dense_lin * inv_second)).astype(
        jnp.bfloat16
    )
    mix_gate = jax.nn.sigmoid(mix_pre * inv_second[:, 0])
    dense_part = (
        jnp.dot(dense_hidden, w_dense_down, preferred_element_type=jnp.float32) * mix_gate[:, None]
    )
    slot_count = CAP * ep_count
    expert_ids = (route_group[:, None] * EPG + route_inner).reshape(-1)
    expert_onehot = (expert_ids[:, None] == jnp.arange(EXPERTS, dtype=jnp.int32)[None, :]).astype(
        jnp.int32
    )
    per_block = expert_onehot.reshape(ep_count, seq_local * TOPK, EXPERTS)
    earlier = (jnp.cumsum(per_block, axis=1) - per_block).reshape(-1, EXPERTS)
    slot_rank = jnp.sum(earlier * expert_onehot, axis=1)
    route_index = jnp.arange(batch_all * TOPK, dtype=jnp.int32)
    block_of = route_index // (seq_local * TOPK)
    slot_flat = expert_ids * slot_count + block_of * CAP + slot_rank
    slot_table = (
        jnp.full((EXPERTS * slot_count,), batch_all, jnp.int32)
        .at[slot_flat]
        .set(route_index // TOPK)
    )
    padded_middle = jnp.concatenate([middle, jnp.zeros((1, col_width), jnp.bfloat16)], axis=0)
    outgoing = jnp.take(padded_middle, slot_table, axis=0).reshape(EXPERTS, slot_count, col_width)
    arrived_float = lax.all_to_all(outgoing, "ep", split_axis=0, concat_axis=2, tiled=True).astype(
        jnp.float32
    )
    inv_rows = lax.rsqrt(jnp.mean(arrived_float * arrived_float, axis=2, keepdims=True) + norm_eps)
    scaled_rows = (arrived_float * gain_float).astype(jnp.bfloat16)
    gate_pre = (
        jnp.einsum("end,edf->enf", scaled_rows, w_exp_gate, preferred_element_type=jnp.float32)
        * inv_rows
    )
    up_proj = (
        jnp.einsum("end,edf->enf", scaled_rows, w_exp_up, preferred_element_type=jnp.float32)
        * inv_rows
    )
    hidden = (jax.nn.silu(gate_pre) * up_proj).astype(jnp.bfloat16)
    expert_rows = jnp.einsum("enf,efd->end", hidden, w_exp_down, preferred_element_type=jnp.float32)
    returned = lax.all_to_all(expert_rows, "ep", split_axis=2, concat_axis=0, tiled=True)
    flat_back = returned.reshape(EXPERTS * slot_count, col_width)
    routed = jnp.take(flat_back, slot_flat, axis=0).reshape(batch_all, TOPK, col_width)
    expert_part = jnp.sum(routed * route_weight[:, :, None], axis=1)
    result_sum = middle_float + lax.psum(expert_part + dense_part, "tp")
    return (result_sum.astype(jnp.bfloat16), new_keys, new_values)


def solution(mesh):
    placed = (
        P(None, "ep"),
        P("ep"),
        P("ep", "tp"),
        P("ep", "tp"),
        P("ep", "tp"),
        P("tp", "ep"),
        P("ep", None, "tp"),
        P("ep", None, "tp"),
        P("ep"),
        P("tp"),
        P(),
        P("ep"),
        P("ep", "tp"),
        P("ep", "tp"),
        P("tp", "ep"),
        P(),
        P(),
        P(),
        P("ep", None, "tp"),
        P("ep", None, "tp"),
        P("ep", "tp", None),
    )
    return jax.shard_map(
        on_device,
        mesh=mesh,
        in_specs=placed,
        out_specs=(P(None, "ep"), P("ep", "tp"), P("ep", "tp")),
        check_vma=False,
    )
```

profile of v0, /device:TPU:0, one launch (start us, length us, event | category | flops | bytes accessed | tf_op | source)
XLA Modules:
  0.0 316.2 jit_solution(12506751394663622789)
XLA Ops:
  8.0 2.5 fusion.3
  10.6 1.0 fusion.14
  11.7 12.3 %copy.64 = bf16[16,1024,256]{1,2,0:T(8,128)(2,1)} copy(bf16[16,1024,256]{2,1,0:T(8,128)(2,1)} %param.27) | data formatting | bytes 16777216 | tf_op jit(solution)/shard_map/reshape | solution.py:65
  26.2 1.0 scatter_custom_fusion
  27.2 11.5 %all-reduce.1 = f32[64]{0:T(128)S(1)} all-reduce(f32[64]{0:T(128)S(1)} %fusion.14), channel_id=3, replica_groups=mesh['ep'=4,'tp'=8] {'ep'}, use_global_device_ids=true, to_apply=%region_2.0.clone | all-reduce | flops 64 | bytes 512
  40.3 4.6 %fusion.58 = f32[16,2,1,1024]{3,2,1,0:T(1,128)S(1)} fusion(bf16[16,2,128,1]{2,3,1,0:T(2,128)(2,1)S(1)} %reshape.226, bf16[16,1024,2,128]{1,3,2,0:T(8,128)(2,1)} %bitcast.59), kind=kOutput, calls=%fused_computation.104 | convolution fusion | flops 8388608 | bytes 8527872 | tf_op jit(solution)/shard_map/bhd,blhd->bhl/dot_general | solution.py:66
  45.4 39.6 %reduce-window.6 = f32[16,2,8,128]{3,2,1,0:T(8,128)S(1)} reduce-window(f32[16,2,8,128]{3,2,1,0:T(8,128)S(1)} %reshape.188, f32[]{:T(128)} %constant.94.clone.1), window={size=1x1x1x128 pad=0_0x0_0x0_0x0_127}, to_apply=%region_3.4 | reduce-window | flops 4161536 | bytes 262148 | tf_op jit(solution)/shard_map/reduce-window
  86.4 4.6 %fusion = f32[16,2,1,128]{3,2,1,0:T(1,128)S(1)} fusion(bf16[16,2,1024,1]{2,1,0,3:T(2,128)(2,1)S(1)} %fusion.42, bf16[16,1024,256]{2,1,0:T(8,128)(2,1)} %param.28), kind=kOutput, calls=%fused_computation.3 | convolution fusion | flops 8388608 | bytes 8470528 | tf_op jit(solution)/shard_map/bhl,blhd->bhd/dot_general | solution.py:77
  91.0 7.1 %all_gather.3 = bf16[64,256]{1,0:T(8,128)(2,1)S(1)} all-gather(bf16[16,256]{1,0:T(8,128)(2,1)S(1)} %bitcast.70), channel_id=1, replica_groups=mesh['ep'=4,'tp'=8] {'ep'}, dimensions={0}, use_global_device_ids=true | all-gather | bytes 40960 | tf_op jit(solution)/shard_map/all_gather | solution.py:80
  98.1 0.9 fusion.59
  99.2 55.8 %all-reduce.8.cloned.1.call-done = f32[64,1024]{1,0:T(8,128)} async-done(((f32[64,1024]{1,0:T(8,128)}), f32[64,1024]{1,0:T(8,128)}) %all-reduce.8.cloned.1.call-update) | async-done | bytes 262160 | tf_op jit(solution)/shard_map/psum | solution.py:84
  154.9 1.1 fusion.17
  156.0 1.2 gather_fusion
  158.1 3.6 %all-to-all-start = ((bf16[16,16,1024]{2,1,0:T(8,128)(2,1)}), bf16[16,16,1024]{2,1,0:T(8,128)(2,1)S(1)}, u32[]{:S(2)}, u32[]{:S(2)}) async-start(bf16[16,16,1024]{2,1,0:T(8,128)(2,1)} %broadcast_select_fusion), calls=%async_computation.1 | async-start | bytes 1048576 | tf_op jit(solution)/shard_map/all_to_all | solution.py:125
  162.3 6.1 %all-to-all-done = bf16[16,16,1024]{2,1,0:T(8,128)(2,1)S(1)} async-done(((bf16[16,16,1024]{2,1,0:T(8,128)(2,1)}), bf16[16,16,1024]{2,1,0:T(8,128)(2,1)S(1)}, u32[]{:S(2)}, u32[]{:S(2)}) %all-to-all-start) | async-done | bytes 524320 | tf_op jit(solution)/shard_map/all_to_all | solution.py:125
  168.4 1.5 copy.82
  169.8 1.9 reshape.192
  172.0 4.5 %convolution_multiply_fusion.2 = f32[4,16,256]{2,1,0:T(8,128)S(1)} fusion(bf16[4,4096,256]{2,1,0:T(8,128)(2,1)} %param.39, f32[4,16,4096]{2,1,0:T(8,128)S(1)} %reshape.192, f32[4096]{0:T(1024)S(1)} %convert_element_type.81, f32[4,16]{1,0:T(4,128)S(1)} %add_rsqrt_fusion), kind=kOutput, calls=%fused_computation.16 | convolution fusion | flops 134758400 | bytes 9519360 | tf_op jit(solution)/shard_map/end,edf->enf/dot_general | solution.py:131
  176.5 8.1 %fusion.12 = f32[4,16,4096]{2,1,0:T(8,128)S(1)} fusion(bf16[4,256,4096]{2,1,0:T(8,128)(2,1)} %param.41, bf16[4,4096,256]{2,1,0:T(8,128)(2,1)} %param.40, f32[4,16,4096]{2,1,0:T(8,128)S(1)} %reshape.192, f32[4096]{0:T(1024)S(1)} %convert_element_type.81, f32[4,16,256]{2,1,0:T(8,128)S(1)} %convolution_multiply_fusion.2, f32[4,16]{1,0:T(4,128)S(1)} %add_rsqrt_fusion), kind=kOutput, calls=%fused_computation.22 | convolution fusion | flops 269074432 | bytes 18956544 | tf_op jit(solution)/shard_map/enf,efd->end/dot_general | solution.py:139
  184.6 5.9 %copy.55 = f32[4,16,4096]{1,0,2:T(4,128)} copy(f32[4,16,4096]{2,1,0:T(8,128)S(1)} %fusion.12) | data formatting | bytes 2097152 | tf_op jit(solution)/shard_map/enf,efd->end/dot_general | solution.py:139
  190.5 8.8 %reshape.230 = f32[4,1,65536]{2,1,0:T(1,128)} reshape(f32[4096,4,16]{2,1,0:T(4,128)} %bitcast.60) | data formatting | bytes 2097152
  199.3 3.5 %all-to-all-start.1 = ((f32[4,1,65536]{2,1,0:T(1,128)}), f32[4,1,65536]{2,1,0:T(1,128)S(1)}, u32[]{:S(2)}, u32[]{:S(2)}) async-start(f32[4,1,65536]{2,1,0:T(1,128)} %reshape.230), calls=%async_computation.2 | async-start | bytes 2097152 | tf_op jit(solution)/shard_map/all_to_all | solution.py:140
  202.9 0.9 fusion.30
  203.8 2.2 fusion.32
  206.2 10.6 %all-reduce.2 = (f32[64]{0:T(128)S(1)}, f32[64]{0:T(128)S(1)}) all-reduce(f32[64]{0:T(128)S(1)} %convolution_bitcast_fusion, f32[64]{0:T(128)S(1)} %get-tuple-element.7), channel_id=1, replica_groups=mesh['ep'=4,'tp'=8] {'ep'}, use_global_device_ids=true, to_apply=%region_16.17 | all-reduce | flops 128 | bytes 1024 | tf_op jit(solution)/shard_map/psum | solution.py:90
  217.5 3.7 %reduce.5 = f32[4,65536]{1,0:T(4,128)S(1)} reduce(f32[4,1,65536]{2,1,0:T(1,128)S(1)} %all-to-all-done.1, f32[]{:T(128)} %broadcast.214), dimensions={1}, to_apply=%all_to_all.9.reduce_sub_computation | reduce | bytes 2097156 | tf_op jit(solution)/shard_map/all_to_all | solution.py:140
  221.2 9.1 %reshape.231 = f32[4096,4,16]{2,1,0:T(4,128)} reshape(f32[4,65536]{1,0:T(4,128)S(1)} %reduce.5) | data formatting | bytes 2097152
  230.3 6.7 %copy.56 = f32[4,16,4,1024]{3,1,0,2:T(8,128)S(1)} copy(f32[4,16,4,1024]{1,0,3,2:T(4,128)} %bitcast.61) | data formatting | bytes 2097152 | tf_op jit(solution)/shard_map/all_to_all | solution.py:140
  238.9 11.5 %all-reduce.12.cloned.1.call-done = (f32[64,512]{1,0:T(8,128)}, f32[64,512]{1,0:T(8,128)}) async-done(((f32[64,512]{1,0:T(8,128)}, f32[64,512]{1,0:T(8,128)}), (f32[64,512]{1,0:T(8,128)}, f32[64,512]{1,0:T(8,128)})) %all-reduce.12.cloned.1.call-update) | async-done | bytes 262160 | tf_op jit(solution)/shard_map/psum | solution.py:90
  250.4 2.0 fusion.9
  252.5 55.6 %all-reduce.10.cloned.1.call-done = f32[64,1024]{1,0:T(8,128)} async-done(((f32[64,1024]{1,0:T(8,128)}), f32[64,1024]{1,0:T(8,128)}) %all-reduce.10.cloned.1.call-update) | async-done | bytes 262160 | tf_op jit(solution)/shard_map/psum | solution.py:144
  308.1 1.6 fusion.18
  (87 shorter events, 10.3 us)
Async XLA Ops:
  7.2 243.3 %copy-start = (bf16[512,1024]{1,0:T(8,128)(2,1)S(1)}, bf16[512,1024]{1,0:T(8,128)(2,1)}, u32[]{:S(2)}) copy-start(bf16[512,1024]{1,0:T(8,128)(2,1)} %param.35) | copy-start | bytes 3145732
  7.2 31.6 %reduce-scatter.2.cloned.1.call-start = ((), (), s32[]{:S(2)}) async-start(), calls=%async_computation.3 | async-start | bytes 245760 | tf_op jit(solution)/shard_map/reduce_scatter | solution.py:52
  10.5 144.4 %all-reduce.8.cloned.1.call-start = ((), (), s32[]{:S(2)}) async-start(), calls=%async_computation.4 | async-start | bytes 524288 | tf_op jit(solution)/shard_map/psum | solution.py:84
  11.6 12.3 %copy-start.10 = (s32[64]{0:T(128)S(1)}, s32[64]{0:T(128)}, u32[]{:S(2)}) copy-start(s32[64]{0:T(128)} %param.36) | copy-start | bytes 772
  11.6 12.3 %copy-start.8 = (s32[64,2]{0,1:T(2,128)S(1)}, s32[64,2]{0,1:T(2,128)}, u32[]{:S(2)}) copy-start(s32[64,2]{0,1:T(2,128)} %param.37) | copy-start | bytes 1540
  11.6 13.3 %copy-start.11 = (u32[32]{0:T(128)S(1)}, u32[32]{0:T(128)}, u32[]{:S(2)}) copy-start(u32[32]{0:T(128)} %constant.122) | copy-start | bytes 388
  24.0 20.9 %copy-start.5 = (s32[16]{0:T(128)S(1)}, s32[16]{0:T(128)}, u32[]{:S(2)}) copy-start(s32[16]{0:T(128)} %param.29) | copy-start | bytes 196
  24.0 20.9 %copy-start.6 = (f32[2]{0:T(128)S(1)}, f32[2]{0:T(128)}, u32[]{:S(2)}) copy-start(f32[2]{0:T(128)} %param.30) | copy-start | bytes 28
  44.9 53.3 %copy-start.3 = (bf16[256,1024]{1,0:T(8,128)(2,1)S(1)}, bf16[256,1024]{1,0:T(8,128)(2,1)}, u32[]{:S(2)}) copy-start(bf16[256,1024]{1,0:T(8,128)(2,1)} %param.26) | copy-start | bytes 1572868
  44.9 110.1 %copy-start.2 = (bf16[64,1024]{1,0:T(8,128)(2,1)S(1)}, bf16[64,1024]{1,0:T(8,128)(2,1)}, u32[]{:S(2)}) copy-start(bf16[64,1024]{1,0:T(8,128)(2,1)} %param.21) | copy-start | bytes 393220
  86.3 75.5 %copy-start.4 = (bf16[4096]{0:T(1024)(128)(2,1)S(1)}, bf16[4096]{0:T(1024)(128)(2,1)}, u32[]{:S(2)}) copy-start(bf16[4096]{0:T(1024)(128)(2,1)} %param.31) | copy-start | bytes 24580
  86.4 75.8 %copy-start.9 = (f32[64,2]{0,1:T(2,128)S(1)}, f32[64,2]{0,1:T(2,128)}, u32[]{:S(2)}) copy-start(f32[64,2]{0,1:T(2,128)} %param.38) | copy-start | bytes 1540
  86.4 75.8 %copy-start.7 = (bf16[1024]{0:T(1024)(128)(2,1)S(1)}, bf16[1024]{0:T(1024)(128)(2,1)}, u32[]{:S(2)}) copy-start(bf16[1024]{0:T(1024)(128)(2,1)} %param.32) | copy-start | bytes 6148
  158.1 10.3 %all-to-all-start = ((bf16[16,16,1024]{2,1,0:T(8,128)(2,1)}), bf16[16,16,1024]{2,1,0:T(8,128)(2,1)S(1)}, u32[]{:S(2)}, u32[]{:S(2)}) async-start(bf16[16,16,1024]{2,1,0:T(8,128)(2,1)} %broadcast_select_fusion), calls=%async_computation.1 | async-start | bytes 1048576 | tf_op jit(solution)/shard_map/all_to_all | solution.py:125
  184.6 18.2 %copy-start.1 = (bf16[1024,512]{1,0:T(8,128)(2,1)S(1)}, bf16[1024,512]{1,0:T(8,128)(2,1)}, u32[]{:S(2)}) copy-start(bf16[1024,512]{1,0:T(8,128)(2,1)} %param.34) | copy-start | bytes 3145732
  199.3 17.6 %all-to-all-start.1 = ((f32[4,1,65536]{2,1,0:T(1,128)}), f32[4,1,65536]{2,1,0:T(1,128)S(1)}, u32[]{:S(2)}, u32[]{:S(2)}) async-start(f32[4,1,65536]{2,1,0:T(1,128)} %reshape.230), calls=%async_computation.2 | async-start | bytes 2097152 | tf_op jit(solution)/shard_map/all_to_all | solution.py:140
  202.8 47.6 %all-reduce.12.cloned.1.call-start = ((), (), s32[]{:S(2)}) async-start(), calls=%async_computation.6 | async-start | bytes 524288 | tf_op jit(solution)/shard_map/psum | solution.py:90
  206.0 102.0 %all-reduce.10.cloned.1.call-start = ((), (), s32[]{:S(2)}) async-start(), calls=%async_computation.5 | async-start | bytes 524288 | tf_op jit(solution)/shard_map/psum | solution.py:144
Sparse Core Ops, SparseCore 0:
  10.7 26.9 reduce-scatter.1
  99.2 55.6 all-reduce.7
  207.1 43.2 all-reduce.11
  252.6 55.4 all-reduce.9
where the time goes:
time: 317 us; the launch traced here: 316 us
  waiting for transfers between devices  129 us (41%)
  local copies, waits for them, and re-layouts  52.7 us (17%)
  other arithmetic  52.6 us (17%)
  matrix products  30.5 us (10%)
  blocking collectives  29.3 us (9%)
  between operations  14.8 us (5%)
  starting transfers between devices  7.33 us (2%)
    psum x1, waiting for transfers between devices, on_device(): attn_out = lax.psum(attn_part, 'tp')  55.8 us
    psum x1, waiting for transfers between devices, on_device(): result_sum = middle_float + lax.psum(expert_part + dense_part, 'tp')  55.6 us
    another operation x3, other arithmetic  40.5 us
    unnamed x30, local copies, waits for them, and re-layouts  18.6 us
    reshape x1, local copies, waits for them, and re-layouts, on_device(): head_keys = key_cache.reshape(seq_local, cache_len, heads_local, HD)  12.3 us
    psum x1, waiting for transfers between devices, on_device(): lax.psum((jnp.dot(scaled_mid, w_dense_gate, preferred_element_type=jnp.fl...  11.5 us
    unnamed x1, blocking collectives  11.5 us
    psum x1, blocking collectives, on_device(): lax.psum((jnp.dot(scaled_mid, w_dense_gate, preferred_element_type=jnp.fl...  10.6 us
  transfers between devices with their start and end apart: 6, of which 4 were waited for; matrix products, arithmetic and copies ran while one was open for 13% of the time, Pallas kernels for 0%

commit v1 on v0

--- a/solution.py
+++ b/solution.py
@@ -81,7 +81,7 @@
         w_output,
         preferred_element_type=jnp.float32,
     )
-    attn_out = lax.psum(attn_part, "tp")
+    attn_out = jnp.sum(lax.all_gather(attn_part, "tp"), axis=0)
     middle = (tokens_float + attn_out).astype(jnp.bfloat16)
     middle_float = middle.astype(jnp.float32)
     gain_float = gain_ffn.astype(jnp.float32)

time: 317 us -> 293 us (0.924)
  waiting for transfers between devices: 129 us -> 100 us
  blocking collectives: 29.3 us -> 34 us
    psum x1 -> x0, waiting for transfers between devices: 55.8 us -> none  [on_device(): attn_out = lax.psum(attn_part, 'tp')]
    all_gather x0 -> x1, waiting for transfers between devices: none -> 27.2 us  [on_device(): attn_out = jnp.sum(lax.all_gather(attn_part, 'tp'), axis=0)]
    psum x1, waiting for transfers between devices: 11.5 us -> 7.72 us  [on_device(): lax.psum((jnp.dot(scaled_mid, w_dense_gate, preferred_element_type=jnp.fl...]
    psum x1, blocking collectives: 10.6 us -> 14.4 us  [on_device(): lax.psum((jnp.dot(scaled_mid, w_dense_gate, preferred_element_type=jnp.fl...]
  transfers between devices with their start and end apart: 6 -> 6, of which waited for: 4 -> 5; matrix products, arithmetic and copies ran while one was open for 13% -> 14% of each run, Pallas kernels for 0% -> 0%
where the time goes in v1:
time: 293 us; the launch traced here: 292 us
  waiting for transfers between devices  100 us (34%)
  local copies, waits for them, and re-layouts  52.7 us (18%)
  other arithmetic  52.5 us (18%)
  blocking collectives  34 us (12%)
  matrix products  30.5 us (10%)
  between operations  14.8 us (5%)
  starting transfers between devices  7.33 us (3%)
    psum x1, waiting for transfers between devices, on_device(): result_sum = middle_float + lax.psum(expert_part + dense_part, 'tp')  55.6 us
    another operation x3, other arithmetic  40.5 us
    all_gather x1, waiting for transfers between devices, on_device(): attn_out = jnp.sum(lax.all_gather(attn_part, 'tp'), axis=0)  27.2 us
    unnamed x30, local copies, waits for them, and re-layouts  18.6 us
    psum x1, blocking collectives, on_device(): lax.psum((jnp.dot(scaled_mid, w_dense_gate, preferred_element_type=jnp.fl...  14.4 us
    reshape x1, local copies, waits for them, and re-layouts, on_device(): head_keys = key_cache.reshape(seq_local, cache_len, heads_local, HD)  12.3 us
    unnamed x1, blocking collectives  11.4 us
    all_gather x1, blocking collectives, on_device(): lax.all_gather(attended, 'ep', axis=0, tiled=True)  8.16 us
  transfers between devices with their start and end apart: 6, of which 5 were waited for; matrix products, arithmetic and copies ran while one was open for 14% of the time, Pallas kernels for 0%

profile of v1, /device:TPU:0, one launch (start us, length us, event | category | flops | bytes accessed | tf_op | source)
XLA Modules:
  0.0 292.3 jit_solution(13871883810690784223)
XLA Ops:
  8.0 2.5 fusion.3
  10.6 12.3 %copy.64 = bf16[16,1024,256]{1,2,0:T(8,128)(2,1)} copy(bf16[16,1024,256]{2,1,0:T(8,128)(2,1)} %param.27) | data formatting | bytes 16777216 | tf_op jit(solution)/shard_map/reshape | solution.py:65
  24.3 11.4 %all-reduce.1 = f32[64]{0:T(128)S(1)} all-reduce(f32[64]{0:T(128)S(1)} %fusion.14), channel_id=4, replica_groups=mesh['ep'=4,'tp'=8] {'ep'}, use_global_device_ids=true, to_apply=%region_2.0.clone | all-reduce | flops 64 | bytes 512
  35.8 1.9 reduce-scatter.2.cloned.1.call-done
  39.2 4.6 %fusion.58 = f32[16,2,1,1024]{3,2,1,0:T(1,128)S(1)} fusion(bf16[16,2,128,1]{2,3,1,0:T(2,128)(2,1)S(1)} %reshape.227, bf16[16,1024,2,128]{1,3,2,0:T(8,128)(2,1)} %bitcast.60), kind=kOutput, calls=%fused_computation.104 | convolution fusion | flops 8388608 | bytes 8527872 | tf_op jit(solution)/shard_map/bhd,blhd->bhl/dot_general | solution.py:66
  44.4 39.6 %reduce-window.6 = f32[16,2,8,128]{3,2,1,0:T(8,128)S(1)} reduce-window(f32[16,2,8,128]{3,2,1,0:T(8,128)S(1)} %reshape.188, f32[]{:T(128)} %constant.94.clone.1), window={size=1x1x1x128 pad=0_0x0_0x0_0x0_127}, to_apply=%region_3.4 | reduce-window | flops 4161536 | bytes 262148 | tf_op jit(solution)/shard_map/reduce-window
  85.4 4.6 %fusion = f32[16,2,1,128]{3,2,1,0:T(1,128)S(1)} fusion(bf16[16,2,1024,1]{2,1,0,3:T(2,128)(2,1)S(1)} %fusion.42, bf16[16,1024,256]{2,1,0:T(8,128)(2,1)} %param.28), kind=kOutput, calls=%fused_computation.3 | convolution fusion | flops 8388608 | bytes 8470528 | tf_op jit(solution)/shard_map/bhl,blhd->bhd/dot_general | solution.py:77
  90.0 8.2 %all_gather.9 = bf16[64,256]{1,0:T(8,128)(2,1)S(1)} all-gather(bf16[16,256]{1,0:T(8,128)(2,1)S(1)} %bitcast.72), channel_id=1, replica_groups=mesh['ep'=4,'tp'=8] {'ep'}, dimensions={0}, use_global_device_ids=true | all-gather | bytes 40960 | tf_op jit(solution)/shard_map/all_gather | solution.py:80
  98.1 0.9 fusion.59
  100.1 1.0 scatter_custom_fusion
  101.2 27.2 %all-gather.3.cloned.1.call-done = f32[512,1024]{1,0:T(8,128)} async-done(((f32[64,1024]{1,0:T(8,128)}), f32[512,1024]{1,0:T(8,128)}) %all-gather.3.cloned.1.call-update) | async-done | bytes 2097168 | tf_op jit(solution)/shard_map/all_gather | solution.py:84
  128.4 1.7 reduce_sum.66
  130.3 1.2 gather_fusion
  132.4 3.6 %all-to-all-start = ((bf16[16,16,1024]{2,1,0:T(8,128)(2,1)}), bf16[16,16,1024]{2,1,0:T(8,128)(2,1)S(1)}, u32[]{:S(2)}, u32[]{:S(2)}) async-start(bf16[16,16,1024]{2,1,0:T(8,128)(2,1)} %broadcast_select_fusion), calls=%async_computation.1 | async-start | bytes 1048576 | tf_op jit(solution)/shard_map/all_to_all | solution.py:125
  136.5 8.0 %all-to-all-done = bf16[16,16,1024]{2,1,0:T(8,128)(2,1)S(1)} async-done(((bf16[16,16,1024]{2,1,0:T(8,128)(2,1)}), bf16[16,16,1024]{2,1,0:T(8,128)(2,1)S(1)}, u32[]{:S(2)}, u32[]{:S(2)}) %all-to-all-start) | async-done | bytes 524320 | tf_op jit(solution)/shard_map/all_to_all | solution.py:125
  144.5 1.5 copy.82
  146.0 1.9 reshape.192
  148.1 4.5 %convolution_multiply_fusion.2 = f32[4,16,256]{2,1,0:T(8,128)S(1)} fusion(bf16[4,4096,256]{2,1,0:T(8,128)(2,1)} %param.39, f32[4,16,4096]{2,1,0:T(8,128)S(1)} %reshape.192, f32[4096]{0:T(1024)S(1)} %convert_element_type.81, f32[4,16]{1,0:T(4,128)S(1)} %add_rsqrt_fusion), kind=kOutput, calls=%fused_computation.16 | convolution fusion | flops 134758400 | bytes 9519360 | tf_op jit(solution)/shard_map/end,edf->enf/dot_general | solution.py:131
  152.6 8.1 %fusion.12 = f32[4,16,4096]{2,1,0:T(8,128)S(1)} fusion(bf16[4,256,4096]{2,1,0:T(8,128)(2,1)} %param.41, bf16[4,4096,256]{2,1,0:T(8,128)(2,1)} %param.40, f32[4,16,4096]{2,1,0:T(8,128)S(1)} %reshape.192, f32[4096]{0:T(1024)S(1)} %convert_element_type.81, f32[4,16,256]{2,1,0:T(8,128)S(1)} %convolution_multiply_fusion.2, f32[4,16]{1,0:T(4,128)S(1)} %add_rsqrt_fusion), kind=kOutput, calls=%fused_computation.22 | convolution fusion | flops 269074432 | bytes 18956544 | tf_op jit(solution)/shard_map/enf,efd->end/dot_general | solution.py:139
  160.7 5.9 %copy.55 = f32[4,16,4096]{1,0,2:T(4,128)} copy(f32[4,16,4096]{2,1,0:T(8,128)S(1)} %fusion.12) | data formatting | bytes 2097152 | tf_op jit(solution)/shard_map/enf,efd->end/dot_general | solution.py:139
  166.6 8.8 %reshape.231 = f32[4,1,65536]{2,1,0:T(1,128)} reshape(f32[4096,4,16]{2,1,0:T(4,128)} %bitcast.61) | data formatting | bytes 2097152
  175.4 3.5 %all-to-all-start.1 = ((f32[4,1,65536]{2,1,0:T(1,128)}), f32[4,1,65536]{2,1,0:T(1,128)S(1)}, u32[]{:S(2)}, u32[]{:S(2)}) async-start(f32[4,1,65536]{2,1,0:T(1,128)} %reshape.231), calls=%async_computation.2 | async-start | bytes 2097152 | tf_op jit(solution)/shard_map/all_to_all | solution.py:140
  179.0 0.9 fusion.30
  179.9 2.2 fusion.32
  182.3 14.4 %all-reduce.2 = (f32[64]{0:T(128)S(1)}, f32[64]{0:T(128)S(1)}) all-reduce(f32[64]{0:T(128)S(1)} %convolution_bitcast_fusion, f32[64]{0:T(128)S(1)} %get-tuple-element.7), channel_id=1, replica_groups=mesh['ep'=4,'tp'=8] {'ep'}, use_global_device_ids=true, to_apply=%region_16.17 | all-reduce | flops 128 | bytes 1024 | tf_op jit(solution)/shard_map/psum | solution.py:90
  197.4 3.7 %reduce.5 = f32[4,65536]{1,0:T(4,128)S(1)} reduce(f32[4,1,65536]{2,1,0:T(1,128)S(1)} %all-to-all-done.1, f32[]{:T(128)} %broadcast.214), dimensions={1}, to_apply=%all_to_all.9.reduce_sub_computation | reduce | bytes 2097156 | tf_op jit(solution)/shard_map/all_to_all | solution.py:140
  201.1 9.1 %reshape.232 = f32[4096,4,16]{2,1,0:T(4,128)} reshape(f32[4,65536]{1,0:T(4,128)S(1)} %reduce.5) | data formatting | bytes 2097152
  210.2 6.7 %copy.56 = f32[4,16,4,1024]{3,1,0,2:T(8,128)S(1)} copy(f32[4,16,4,1024]{1,0,3,2:T(4,128)} %bitcast.62) | data formatting | bytes 2097152 | tf_op jit(solution)/shard_map/all_to_all | solution.py:140
  218.8 7.7 %all-reduce.9.cloned.1.call-done = (f32[64,512]{1,0:T(8,128)}, f32[64,512]{1,0:T(8,128)}) async-done(((f32[64,512]{1,0:T(8,128)}, f32[64,512]{1,0:T(8,128)}), (f32[64,512]{1,0:T(8,128)}, f32[64,512]{1,0:T(8,128)})) %all-reduce.9.cloned.1.call-update) | async-done | bytes 262160 | tf_op jit(solution)/shard_map/psum | solution.py:90
  226.5 2.0 fusion.9
  228.5 55.6 %all-reduce.7.cloned.1.call-done = f32[64,1024]{1,0:T(8,128)} async-done(((f32[64,1024]{1,0:T(8,128)}), f32[64,1024]{1,0:T(8,128)}) %all-reduce.7.cloned.1.call-update) | async-done | bytes 262160 | tf_op jit(solution)/shard_map/psum | solution.py:144
  284.1 1.6 fusion.18
  (88 shorter events, 10.6 us)
Async XLA Ops:
  7.2 219.3 %copy-start = (bf16[512,1024]{1,0:T(8,128)(2,1)S(1)}, bf16[512,1024]{1,0:T(8,128)(2,1)}, u32[]{:S(2)}) copy-start(bf16[512,1024]{1,0:T(8,128)(2,1)} %param.35) | copy-start | bytes 3145732
  7.2 30.6 %reduce-scatter.2.cloned.1.call-start = ((), (), s32[]{:S(2)}) async-start(), calls=%async_computation.3 | async-start | bytes 245760 | tf_op jit(solution)/shard_map/reduce_scatter | solution.py:52
  10.5 117.9 %all-gather.3.cloned.1.call-start = ((), (), s32[]{:S(2)}) async-start(), calls=%async_computation.5 | async-start | bytes 2359296 | tf_op jit(solution)/shard_map/all_gather | solution.py:84
  10.6 12.4 %copy-start.11 = (u32[32]{0:T(128)S(1)}, u32[32]{0:T(128)}, u32[]{:S(2)}) copy-start(u32[32]{0:T(128)} %constant.122) | copy-start | bytes 388
  10.6 13.6 %copy-start.2 = (bf16[64,1024]{1,0:T(8,128)(2,1)S(1)}, bf16[64,1024]{1,0:T(8,128)(2,1)}, u32[]{:S(2)}) copy-start(bf16[64,1024]{1,0:T(8,128)(2,1)} %param.21) | copy-start | bytes 393220
  22.9 20.9 %copy-start.5 = (s32[16]{0:T(128)S(1)}, s32[16]{0:T(128)}, u32[]{:S(2)}) copy-start(s32[16]{0:T(128)} %param.29) | copy-start | bytes 196
  22.9 20.9 %copy-start.6 = (f32[2]{0:T(128)S(1)}, f32[2]{0:T(128)}, u32[]{:S(2)}) copy-start(f32[2]{0:T(128)} %param.30) | copy-start | bytes 28
  43.8 54.3 %copy-start.3 = (bf16[256,1024]{1,0:T(8,128)(2,1)S(1)}, bf16[256,1024]{1,0:T(8,128)(2,1)}, u32[]{:S(2)}) copy-start(bf16[256,1024]{1,0:T(8,128)(2,1)} %param.26) | copy-start | bytes 1572868
  43.8 55.3 %copy-start.10 = (s32[64]{0:T(128)S(1)}, s32[64]{0:T(128)}, u32[]{:S(2)}) copy-start(s32[64]{0:T(128)} %param.36) | copy-start | bytes 772
  43.8 55.3 %copy-start.8 = (s32[64,2]{0,1:T(2,128)S(1)}, s32[64,2]{0,1:T(2,128)}, u32[]{:S(2)}) copy-start(s32[64,2]{0,1:T(2,128)} %param.37) | copy-start | bytes 1540
  85.3 50.8 %copy-start.4 = (bf16[4096]{0:T(1024)(128)(2,1)S(1)}, bf16[4096]{0:T(1024)(128)(2,1)}, u32[]{:S(2)}) copy-start(bf16[4096]{0:T(1024)(128)(2,1)} %param.31) | copy-start | bytes 24580
  85.3 51.0 %copy-start.9 = (f32[64,2]{0,1:T(2,128)S(1)}, f32[64,2]{0,1:T(2,128)}, u32[]{:S(2)}) copy-start(f32[64,2]{0,1:T(2,128)} %param.38) | copy-start | bytes 1540
  85.3 51.1 %copy-start.7 = (bf16[1024]{0:T(1024)(128)(2,1)S(1)}, bf16[1024]{0:T(1024)(128)(2,1)}, u32[]{:S(2)}) copy-start(bf16[1024]{0:T(1024)(128)(2,1)} %param.32) | copy-start | bytes 6148
  132.4 12.1 %all-to-all-start = ((bf16[16,16,1024]{2,1,0:T(8,128)(2,1)}), bf16[16,16,1024]{2,1,0:T(8,128)(2,1)S(1)}, u32[]{:S(2)}, u32[]{:S(2)}) async-start(bf16[16,16,1024]{2,1,0:T(8,128)(2,1)} %broadcast_select_fusion), calls=%async_computation.1 | async-start | bytes 1048576 | tf_op jit(solution)/shard_map/all_to_all | solution.py:125
  160.7 18.2 %copy-start.1 = (bf16[1024,512]{1,0:T(8,128)(2,1)S(1)}, bf16[1024,512]{1,0:T(8,128)(2,1)}, u32[]{:S(2)}) copy-start(bf16[1024,512]{1,0:T(8,128)(2,1)} %param.34) | copy-start | bytes 3145732
  175.4 21.3 %all-to-all-start.1 = ((f32[4,1,65536]{2,1,0:T(1,128)}), f32[4,1,65536]{2,1,0:T(1,128)S(1)}, u32[]{:S(2)}, u32[]{:S(2)}) async-start(f32[4,1,65536]{2,1,0:T(1,128)} %reshape.231), calls=%async_computation.2 | async-start | bytes 2097152 | tf_op jit(solution)/shard_map/all_to_all | solution.py:140
  178.9 47.6 %all-reduce.9.cloned.1.call-start = ((), (), s32[]{:S(2)}) async-start(), calls=%async_computation.6 | async-start | bytes 524288 | tf_op jit(solution)/shard_map/psum | solution.py:90
  182.1 102.0 %all-reduce.7.cloned.1.call-start = ((), (), s32[]{:S(2)}) async-start(), calls=%async_computation.4 | async-start | bytes 524288 | tf_op jit(solution)/shard_map/psum | solution.py:144
Sparse Core Ops, SparseCore 0:
  10.7 26.9 reduce-scatter.1
  99.2 29.1 all-gather.2
  183.2 43.2 all-reduce.8
  228.7 55.4 all-reduce.6
